TPU v7x, 32 devices: a whole 2x2x4 slice. The times are simulated.
32 devices in a mesh: fs: 8 (over z, y), tp: 4 (over x, core).
Axes of the slice: x: 2, y: 2, z: 4, core: 2. Of those that a mesh axis runs over, the one named last changes fastest.
Arguments:
- tokens: bfloat16 [8192, 2048], P('fs', 'tp'), may hold values from -6 to 6
- mixer_gain: float32 [2048], replicated, may hold values from 0.1 to 1.9
- ffn_gain: float32 [2048], replicated, may hold values from 0.1 to 1.9
- w_outer: float32 [2048, 1024], P('fs', 'tp'), may hold values from -0.125 to 0.125
- w_inner: float32 [2048, 1024], P('fs', 'tp'), may hold values from -0.125 to 0.125
- w_value: float32 [2048, 1024], P('fs', 'tp'), may hold values from -0.125 to 0.125
- scale_outer: float32 [1, 1024], P(None, 'tp'), may hold values from 0.5 to 2
- scale_inner: float32 [1, 1024], P(None, 'tp'), may hold values from 0.5 to 2
- scale_value: float32 [1, 1024], P(None, 'tp'), may hold values from 0.5 to 2
- conv_taps: float32 [3, 1024], P(None, 'tp'), may hold values from -3.5 to 3.5
- w_mixout: float32 [1024, 2048], P('tp', 'fs'), may hold values from -0.1875 to 0.1875
- scale_mixout: float32 [1, 2048], P(None, 'fs'), may hold values from 0.5 to 2
- w_gate: float32 [2048, 5632], P('fs', 'tp'), may hold values from -0.125 to 0.125
- w_upward: float32 [2048, 5632], P('fs', 'tp'), may hold values from -0.125 to 0.125
- scale_gate: float32 [1, 5632], P(None, 'tp'), may hold values from 0.5 to 2
- scale_upward: float32 [1, 5632], P(None, 'tp'), may hold values from 0.5 to 2
- w_down: float32 [5632, 2048], P('tp', 'fs'), may hold values from -0.078125 to 0.078125
- scale_down: float32 [1, 2048], P(None, 'fs'), may hold values from 0.5 to 2
Outputs:
- block_out: bfloat16 [8192, 2048], P('fs', 'tp')
All inputs are finite; a program needn't handle non-finite values.
Results may differ from a plain program's by a relative error of at most 0.019.
Values may be sent and summed in bfloat16 or wider, within the bound.
A program may use at most 128 MiB of HBM per device.

v0:
```python
import jax
import jax.numpy as jnp
from jax import lax
from jax.sharding import PartitionSpec as P

SEQ_LEN = 128


def rms_scaled(full_rows, gain_vec):
    values = full_rows.astype(jnp.float32)
    inverse = lax.rsqrt(jnp.mean(values * values, axis=-1, keepdims=True) + 1e-06)
    return (values * inverse * gain_vec).astype(jnp.bfloat16)


def add_rows(left, w_piece):
    return jnp.dot(left, w_piece, preferred_element_type=jnp.float32)


def causal_taps(product, conv_taps):
    padded = jnp.pad(product, ((0, 0), (conv_taps.shape[0] - 1, 0), (0, 0)))
    length = product.shape[1]
    summed = jnp.zeros(product.shape, jnp.float32)
    for tap_index in range(conv_taps.shape[0]):
        summed = summed + conv_taps[tap_index] * padded[:, tap_index : tap_index + length, :]
    return summed


def per_device(
    tokens,
    mixer_gain,
    ffn_gain,
    w_outer,
    w_inner,
    w_value,
    scale_outer,
    scale_inner,
    scale_value,
    conv_taps,
    w_mixout,
    scale_mixout,
    w_gate,
    w_upward,
    scale_gate,
    scale_upward,
    w_down,
    scale_down,
):
    full_rows = lax.all_gather(tokens, "tp", axis=1, tiled=True)
    normed = rms_scaled(full_rows, mixer_gain)
    tok_count = tokens.shape[0]
    local_channels = w_outer.shape[1]

    def add_one(w_piece):
        return add_rows(normed, w_piece)

    outer_bf = w_outer.astype(jnp.bfloat16)
    inner_bf = w_inner.astype(jnp.bfloat16)
    value_bf = w_value.astype(jnp.bfloat16)
    outer = add_one(lax.all_gather(outer_bf, "fs", axis=0, tiled=True))
    inner = add_one(lax.all_gather(inner_bf, "fs", axis=0, tiled=True))
    value = add_one(lax.all_gather(value_bf, "fs", axis=0, tiled=True))
    outer = outer * scale_outer
    product = inner * scale_inner * (value * scale_value)
    product = product.reshape(tok_count // SEQ_LEN, SEQ_LEN, local_channels)
    conv = causal_taps(product, conv_taps).reshape(tok_count, local_channels)
    mixed_out = (outer * conv).astype(jnp.bfloat16)
    mixout_scales, down_scales = (
        lax.all_gather(scale_mixout, "fs", axis=1, tiled=True),
        lax.all_gather(scale_down, "fs", axis=1, tiled=True),
    )
    mixout_bf = w_mixout.astype(jnp.bfloat16)
    mixed_all = lax.all_gather(mixed_out, "tp", axis=1, tiled=True)
    mixout_cols = lax.all_gather(mixout_bf, "fs", axis=1, tiled=True)
    mixout_all = lax.all_gather(mixout_cols, "tp", axis=0, tiled=True)
    mix_term = jnp.dot(mixed_all, mixout_all, preferred_element_type=jnp.float32) * mixout_scales
    residual_rows = (full_rows.astype(jnp.float32) + mix_term).astype(jnp.bfloat16)
    feature_count = tokens.shape[1]
    residual = lax.dynamic_slice_in_dim(
        residual_rows, lax.axis_index("tp") * feature_count, feature_count, 1
    )
    normed_ffn = rms_scaled(residual_rows, ffn_gain)
    gate_proj = add_rows(
        normed_ffn, lax.all_gather(w_gate.astype(jnp.bfloat16), "fs", axis=0, tiled=True)
    )
    up_proj = add_rows(
        normed_ffn, lax.all_gather(w_upward.astype(jnp.bfloat16), "fs", axis=0, tiled=True)
    )
    hidden = (jax.nn.silu(gate_proj * scale_gate) * (up_proj * scale_upward)).astype(jnp.bfloat16)
    down_terms = (
        jnp.dot(
            hidden,
            lax.all_gather(w_down.astype(jnp.bfloat16), "fs", axis=1, tiled=True),
            preferred_element_type=jnp.float32,
        )
        * down_scales
    )
    ffn_share = lax.psum_scatter(
        down_terms.astype(jnp.bfloat16), "tp", scatter_dimension=1, tiled=True
    ).astype(jnp.float32)
    return (residual.astype(jnp.float32) + ffn_share).astype(jnp.bfloat16)


def solution(mesh):
    in_specs = (
        P("fs", "tp"),
        P(),
        P(),
        P("fs", "tp"),
        P("fs", "tp"),
        P("fs", "tp"),
        P(None, "tp"),
        P(None, "tp"),
        P(None, "tp"),
        P(None, "tp"),
        P("tp", "fs"),
        P(None, "fs"),
        P("fs", "tp"),
        P("fs", "tp"),
        P(None, "tp"),
        P(None, "tp"),
        P("tp", "fs"),
        P(None, "fs"),
    )
    out_specs = P("fs", "tp")
    return jax.shard_map(
        per_device, mesh=mesh, in_specs=in_specs, out_specs=out_specs, check_vma=False
    )
```

profile of v0, /device:TPU:0, one launch (start us, length us, event | category | flops | bytes accessed | tf_op | source)
XLA Modules:
  0.0 623.6 jit_solution(6061713341310638662)
XLA Ops:
  6.5 1.6 convert_element_type.63
  8.2 0.7 all-gather.11.cloned.1.call-update
  9.0 1.6 convert_element_type.61
  10.6 0.0 all-gather.15.cloned.1.call-start
  10.7 1.6 convert_element_type.60
  12.4 1.6 convert_element_type.59
  14.0 37.5 %all-gather.21.cloned.1.call-done = bf16[256,2048]{1,0:T(8,128)(2,1)} async-done(((bf16[256,256]{1,0:T(8,128)(2,1)}), bf16[256,2048]{1,0:T(8,128)(2,1)}) %all-gather.21.cloned.1.call-update) | async-done | bytes 1048592 | tf_op jit(solution)/shard_map/all_gather | solution.py:73
  51.6 0.8 fusion.20
  52.4 34.2 %all-gather.11.cloned.1.call-done = bf16[1024,2048]{1,0:T(8,128)(2,1)} async-done(((bf16[1024,512]{1,0:T(8,128)(2,1)}), bf16[1024,2048]{1,0:T(8,128)(2,1)}) %all-gather.11.cloned.1.call-update) | async-done | bytes 4194320 | tf_op jit(solution)/shard_map/all_gather | solution.py:48
  86.6 3.1 fusion.3
  89.7 39.4 %all-gather.17.cloned.1.call-done = bf16[2048,256]{1,0:T(8,128)(2,1)} async-done(((bf16[256,256]{1,0:T(8,128)(2,1)}), bf16[2048,256]{1,0:T(8,128)(2,1)}) %all-gather.17.cloned.1.call-update) | async-done | bytes 1048592 | tf_op jit(solution)/shard_map/all_gather | solution.py:61
  129.0 3.8 convolution_multiply_fusion
  132.9 37.2 %all-gather.15.cloned.1.call-done = bf16[2048,256]{1,0:T(8,128)(2,1)} async-done(((bf16[256,256]{1,0:T(8,128)(2,1)}), bf16[2048,256]{1,0:T(8,128)(2,1)}) %all-gather.15.cloned.1.call-update) | async-done | bytes 1048592 | tf_op jit(solution)/shard_map/all_gather | solution.py:60
  170.0 3.8 fusion.8
  173.9 1.3 fusion.15
  175.2 35.9 %all-gather.13.cloned.1.call-done = bf16[2048,256]{1,0:T(8,128)(2,1)} async-done(((bf16[256,256]{1,0:T(8,128)(2,1)}), bf16[2048,256]{1,0:T(8,128)(2,1)}) %all-gather.13.cloned.1.call-update) | async-done | bytes 1048592 | tf_op jit(solution)/shard_map/all_gather | solution.py:59
  211.0 5.1 fusion.9
  216.2 1.0 convert_element_type.68
  217.2 0.0 all-gather.27.cloned.1.call-start
  217.3 1.0 convert_element_type.69
  218.3 2.5 convert_element_type.71
  220.9 18.2 %all_gather.43 = f32[1,2048]{1,0:T(1,128)S(1)} all-gather(f32[1,256]{1,0:T(1,128)S(1)} %copy-done.4), channel_id=1, replica_groups=mesh['fs'=8,'tp'=4] {'fs'}, dimensions={1}, use_global_device_ids=true | all-gather | bytes 9216 | tf_op jit(solution)/shard_map/all_gather | solution.py:68
  239.1 16.6 %all_gather.47 = f32[1,2048]{1,0:T(1,128)S(1)} all-gather(f32[1,256]{1,0:T(1,128)S(1)} %copy-done.5), channel_id=1, replica_groups=mesh['fs'=8,'tp'=4] {'fs'}, dimensions={1}, use_global_device_ids=true | all-gather | bytes 9216 | tf_op jit(solution)/shard_map/all_gather | solution.py:69
  255.7 14.3 %all-gather.19.cloned.1.call-done = bf16[1024,1024]{1,0:T(8,128)(2,1)} async-done(((bf16[1024,256]{1,0:T(8,128)(2,1)}), bf16[1024,1024]{1,0:T(8,128)(2,1)}) %all-gather.19.cloned.1.call-update) | async-done | bytes 2097168 | tf_op jit(solution)/shard_map/all_gather | solution.py:72
  270.1 10.9 %fusion = (f32[1024]{0:T(1024)S(1)}, bf16[1024,2048]{1,0:T(8,128)(2,1)}) fusion(f32[2048]{0:T(1024)S(1)} %bitcast.26, bf16[1024,1024]{1,0:T(8,128)(2,1)} %all-gather.19.cloned.1.call-done, bf16[1024,2048]{1,0:T(8,128)(2,1)} %all-gather.23.cloned.1.call-done, bf16[1024,2048]{1,0:T(8,128)(2,1)} %all-gather.11.cloned.1.call-done), kind=kOutput, calls=%fused_computation.5 | convolution fusion | flops 4309646336 | bytes 14692352 | tf_op jit(solution)/shard_map/dot_general | solution.py:75
  281.0 83.6 %all-gather.25.cloned.1.call-done = bf16[2048,1408]{1,0:T(8,128)(2,1)} async-done(((bf16[256,1408]{1,0:T(8,128)(2,1)}), bf16[2048,1408]{1,0:T(8,128)(2,1)}) %all-gather.25.cloned.1.call-update) | async-done | bytes 5767184 | tf_op jit(solution)/shard_map/all_gather | solution.py:83
  364.6 11.9 %fusion.11 = f32[1024,1408]{1,0:T(8,128)} fusion(bf16[2048,1408]{1,0:T(8,128)(2,1)} %all-gather.25.cloned.1.call-done, bf16[1024,2048]{1,0:T(8,128)(2,1)} %get-tuple-element.9, f32[2048]{0:T(1024)S(1)} %copy-done.7, f32[1024]{0:T(1024)S(1)} %add_rsqrt_fusion), kind=kOutput, calls=%fused_computation.21 | convolution fusion | flops 5913968640 | bytes 15740928 | tf_op jit(solution)/shard_map/dot_general | solution.py:16
  376.5 80.8 %all-gather.27.cloned.1.call-done = bf16[2048,1408]{1,0:T(8,128)(2,1)} async-done(((bf16[256,1408]{1,0:T(8,128)(2,1)}), bf16[2048,1408]{1,0:T(8,128)(2,1)}) %all-gather.27.cloned.1.call-update) | async-done | bytes 5767184 | tf_op jit(solution)/shard_map/all_gather | solution.py:86
  457.3 93.2 %all-gather.29.cloned.1.call-done = bf16[1408,2048]{1,0:T(8,128)(2,1)} async-done(((bf16[1408,256]{1,0:T(8,128)(2,1)}), bf16[1408,2048]{1,0:T(8,128)(2,1)}) %all-gather.29.cloned.1.call-update) | async-done | bytes 5767184 | tf_op jit(solution)/shard_map/all_gather | solution.py:92
  550.5 21.0 %multiply_convert_fusion = bf16[1024,2048]{1,0:T(8,128)(2,1)} fusion(bf16[1408,2048]{1,0:T(8,128)(2,1)} %all-gather.29.cloned.1.call-done, f32[2048]{0:T(1024)S(1)} %bitcast.25, f32[1024,1408]{1,0:T(8,128)} %fusion.11, bf16[2048,1408]{1,0:T(8,128)(2,1)} %all-gather.27.cloned.1.call-done, f32[1408]{0:T(1024)S(1)} %reduce.1, f32[1408]{0:T(1024)S(1)} %reduce, ...), kind=kOutput, calls=%fused_computation.12 | convolution fusion | flops 11835277312 | bytes 25721856 | tf_op jit(solution)/shard_map/dot_general | solution.py:90
  571.6 42.7 %reduce-scatter.2.cloned.1.call-done = bf16[1024,512]{1,0:T(8,128)(2,1)} async-done(((bf16[1024,2048]{1,0:T(8,128)(2,1)}), bf16[1024,512]{1,0:T(8,128)(2,1)}) %reduce-scatter.2.cloned.1.call-update) | async-done | bytes 1048592 | tf_op jit(solution)/shard_map/reduce_scatter | solution.py:97
  614.3 2.8 add_convert_fusion
  (46 shorter events, 0.6 us)
Async XLA Ops:
  6.5 122.5 %copy-start.8 = (f32[1,256]{1,0:T(1,128)S(1)}, f32[1,256]{1,0:T(1,128)}, u32[]{:S(2)}) copy-start(f32[1,256]{1,0:T(1,128)} %param.26) | copy-start | bytes 3076
  6.5 122.5 %copy-start.6 = (f32[2048]{0:T(1024)S(1)}, f32[2048]{0:T(1024)}, u32[]{:S(2)}) copy-start(f32[2048]{0:T(1024)} %param.19) | copy-start | bytes 24580
  6.5 45.0 %all-gather.21.cloned.1.call-start = ((), (), s32[]{:S(2)}) async-start(), calls=%async_computation.6 | async-start | bytes 1179648 | tf_op jit(solution)/shard_map/all_gather | solution.py:73
  8.2 78.4 %all-gather.11.cloned.1.call-start = ((), (), s32[]{:S(2)}) async-start(), calls=%async_computation.1 | async-start | bytes 5242880 | tf_op jit(solution)/shard_map/all_gather | solution.py:48
  8.9 120.1 %all-gather.17.cloned.1.call-start = ((), (), s32[]{:S(2)}) async-start(), calls=%async_computation.4 | async-start | bytes 1179648 | tf_op jit(solution)/shard_map/all_gather | solution.py:61
  10.6 159.4 %all-gather.15.cloned.1.call-start = ((), (), s32[]{:S(2)}) async-start(), calls=%async_computation.3 | async-start | bytes 1179648 | tf_op jit(solution)/shard_map/all_gather | solution.py:60
  12.3 198.7 %all-gather.13.cloned.1.call-start = ((), (), s32[]{:S(2)}) async-start(), calls=%async_computation.2 | async-start | bytes 1179648 | tf_op jit(solution)/shard_map/all_gather | solution.py:59
  14.0 241.7 %all-gather.23.cloned.1.call-start = ((), (), s32[]{:S(2)}) async-start(), calls=%async_computation.7 | async-start | bytes 5242880 | tf_op jit(solution)/shard_map/all_gather | solution.py:74
  51.6 218.5 %all-gather.19.cloned.1.call-start = ((), (), s32[]{:S(2)}) async-start(), calls=%async_computation.5 | async-start | bytes 2621440 | tf_op jit(solution)/shard_map/all_gather | solution.py:72
  129.0 41.0 %copy-start.9 = (f32[1,256]{1,0:T(1,128)S(1)}, f32[1,256]{1,0:T(1,128)}, u32[]{:S(2)}) copy-start(f32[1,256]{1,0:T(1,128)} %param.25) | copy-start | bytes 3076
  170.0 41.0 %copy-start.10 = (f32[1,256]{1,0:T(1,128)S(1)}, f32[1,256]{1,0:T(1,128)}, u32[]{:S(2)}) copy-start(f32[1,256]{1,0:T(1,128)} %param.24) | copy-start | bytes 3076
  211.0 5.2 copy-start
  211.0 6.2 copy-start.1
  216.1 4.7 copy-start.2
  216.1 4.8 copy-start.3
  216.1 4.8 copy-start.4
  216.1 23.0 %copy-start.5 = (f32[1,256]{1,0:T(1,128)S(1)}, f32[1,256]{1,0:T(1,128)}, u32[]{:S(2)}) copy-start(f32[1,256]{1,0:T(1,128)} %param.35) | copy-start | bytes 3076
  216.2 148.4 %all-gather.25.cloned.1.call-start = ((), (), s32[]{:S(2)}) async-start(), calls=%async_computation.8 | async-start | bytes 6488064 | tf_op jit(solution)/shard_map/all_gather | solution.py:83
  217.2 240.1 %all-gather.27.cloned.1.call-start = ((), (), s32[]{:S(2)}) async-start(), calls=%async_computation.9 | async-start | bytes 6488064 | tf_op jit(solution)/shard_map/all_gather | solution.py:86
  218.3 332.3 %all-gather.29.cloned.1.call-start = ((), (), s32[]{:S(2)}) async-start(), calls=%async_computation.10 | async-start | bytes 6488064 | tf_op jit(solution)/shard_map/all_gather | solution.py:92
  220.8 393.5 %reduce-scatter.2.cloned.1.call-start = ((), (), s32[]{:S(2)}) async-start(), calls=%async_computation.11 | async-start | bytes 5242880 | tf_op jit(solution)/shard_map/reduce_scatter | solution.py:97
  270.0 94.5 %copy-start.7 = (f32[2048]{0:T(1024)S(1)}, f32[2048]{0:T(1024)}, u32[]{:S(2)}) copy-start(f32[2048]{0:T(1024)} %param.20) | copy-start | bytes 24580
Sparse Core Ops, SparseCore 0:
  9.4 42.1 all-gather.20
  53.1 33.4 all-gather.10
  88.7 40.2 all-gather.16
  131.0 38.9 all-gather.14
  172.0 38.9 all-gather.12
  212.5 33.1 all-gather.22
  247.2 22.8 all-gather.18
  272.2 92.2 all-gather.24
  366.8 90.4 all-gather.26
  459.2 91.2 all-gather.28
  571.7 42.5 reduce-scatter.1
where the time goes:
time: 624 us
  waiting for transfers between devices  500 us (80%)
  matrix products  56.6 us (9%)
  blocking collectives  34.8 us (6%)
  other arithmetic  18 us (3%)
  between operations  13.3 us (2%)
    all_gather x1, waiting for transfers between devices, per_device(): lax.all_gather(w_down.astype(jnp.bfloat16), 'fs', axis=1, tiled=True)  93.2 us
    all_gather x1, waiting for transfers between devices, per_device(): lax.all_gather(w_gate.astype(jnp.bfloat16), 'fs', axis=0, tiled=True)  83.6 us
    all_gather x1, waiting for transfers between devices, per_device(): lax.all_gather(w_upward.astype(jnp.bfloat16), 'fs', axis=0, tiled=True)  80.8 us
    reduce_scatter x1, waiting for transfers between devices, per_device(): lax.psum_scatter(down_terms.astype(jnp.bfloat16), 'tp', scatter_dimension...  42.7 us
    all_gather x1, waiting for transfers between devices, per_device(): value = add_one(lax.all_gather(value_bf, 'fs', axis=0, tiled=True))  39.4 us
    all_gather x1, waiting for transfers between devices, per_device(): mixout_cols = lax.all_gather(mixout_bf, 'fs', axis=1, tiled=True)  37.5 us
    all_gather x1, waiting for transfers between devices, per_device(): inner = add_one(lax.all_gather(inner_bf, 'fs', axis=0, tiled=True))  37.2 us
    all_gather x1, waiting for transfers between devices, per_device(): outer = add_one(lax.all_gather(outer_bf, 'fs', axis=0, tiled=True))  35.9 us
  transfers between devices with their start and end apart: 11, of which 10 were waited for; matrix products, arithmetic and copies ran while one was open for 8% of the time, Pallas kernels for 0%

commit v1 on v0

--- a/solution.py
+++ b/solution.py
@@ -1,6 +1,8 @@
 import jax
 import jax.numpy as jnp
 from jax import lax
+from jax.experimental import pallas as pl
+from jax.experimental.pallas import tpu as pltpu
 from jax.sharding import PartitionSpec as P
 
 SEQ_LEN = 128
@@ -25,7 +27,311 @@
     return summed
 
 
-def per_device(
+DEPTH, WIDTH, TP = 4, 2, 4
+ROWS = 256
+MESH = pl.DeviceIdType.MESH
+
+
+def block_kernel(
+    tokens, mixer_gain, ffn_gain, s_mixer, taps, s_gate, s_up,
+    h_scales, h_mixer, h_mixout, h_gate, h_up, h_down,
+    out, residual_own,
+    rows, mixer, mixout, gate, up, down, scales, mixed, hidden,
+    fs_send, fs_recv, tp_send, tp_recv, local_sem,
+):
+    f32, bf16 = jnp.float32, jnp.bfloat16
+    me, tp = lax.axis_index("fs"), lax.axis_index("tp")
+    zed, why = lax.div(me, WIDTH), lax.rem(me, WIDTH)
+    near_x, core = lax.div(tp, 2), lax.rem(tp, 2)
+
+    def at(dz, dy):
+        return lax.rem(zed + dz + DEPTH, DEPTH) * WIDTH + lax.rem(why + dy, WIDTH)
+
+    beside, above, below = at(0, 1), at(1, 0), at(-1, 0)
+    sibling = near_x * 2 + (1 - core)
+    across = (1 - near_x) * 2 + core
+
+    barrier = pltpu.get_barrier_semaphore()
+    for peer in (beside, above, below):
+        pl.semaphore_signal(barrier, inc=1, device_id={"fs": peer}, device_id_type=MESH)
+    for peer in (sibling, across):
+        pl.semaphore_signal(barrier, inc=1, device_id={"tp": peer}, device_id_type=MESH)
+    pl.semaphore_wait(barrier, 5)
+
+    shards = (h_scales, h_mixer, h_mixout, h_gate, h_up, h_down)
+    fulls = (scales, mixer, mixout, gate, up, down)
+    by_columns = (False, False, True, False, False, True)
+
+    def slot(w, owner, part):
+        height, wide = shards[w].shape
+        first, size = 0, height
+        if part is not None:
+            size = height // 2
+            first = part * size
+        if by_columns[w]:
+            base = tp * height if w == 2 else 0
+            start = base + first
+            if w == 2:
+                start = pl.multiple_of(start, 128)
+            return fulls[w].at[pl.ds(start, size), pl.ds(pl.multiple_of(owner * wide, wide), wide)]
+        return fulls[w].at[pl.ds(pl.multiple_of(owner * height + first, size), size), :]
+
+    kinds = (
+        ((0, 0), None, beside), ((0, 0), None, above), ((0, 0), None, below),
+        ((0, 1), None, above), ((0, 1), None, below),
+        ((-1, 0), 0, above), ((1, 0), 1, below),
+        ((2, 0), 0, beside), ((2, 0), 1, beside),
+    )
+
+    def copy(w, k):
+        (dz, dy), part, target = kinds[k]
+        place = slot(w, at(dz, dy), part)
+        return pltpu.make_async_remote_copy(
+            src_ref=shards[w] if k < 3 else place,
+            dst_ref=place,
+            send_sem=fs_send.at[w, k],
+            recv_sem=fs_recv.at[w, k],
+            device_id={"fs": target},
+            device_id_type=MESH,
+        )
+
+    def own(w):
+        return pltpu.make_async_copy(shards[w], slot(w, me, None), local_sem.at[w])
+
+    def first(w):
+        for k in (0, 1, 2):
+            copy(w, k).start()
+        own(w).start()
+
+    def second(w):
+        copy(w, 1).wait_recv()
+        copy(w, 5).start()
+        copy(w, 2).wait_recv()
+        copy(w, 6).start()
+        copy(w, 0).wait_recv()
+        copy(w, 3).start()
+        copy(w, 4).start()
+
+    def third(w):
+        copy(w, 5).wait_recv()
+        copy(w, 7).start()
+        copy(w, 6).wait_recv()
+        copy(w, 8).start()
+
+    def finish(w):
+        for k in (3, 4, 7, 8):
+            copy(w, k).wait_recv()
+        own(w).wait()
+
+    def tp_slot(a, owner):
+        if a == 0:
+            wide = tokens.shape[1]
+            return rows.at[:, pl.ds(pl.multiple_of(owner * wide, wide), wide)]
+        if a == 1:
+            wide = mixed.shape[1] // TP
+            return mixed.at[:, pl.ds(pl.multiple_of(owner * wide, wide), wide)]
+        height = mixout.shape[0] // TP
+        return mixout.at[pl.ds(pl.multiple_of(owner * height, height), height), :]
+
+    def tp_copy(a, k):
+        owner, target = ((tp, sibling), (tp, across), (across, sibling))[k]
+        place = tp_slot(a, owner)
+        return pltpu.make_async_remote_copy(
+            src_ref=tokens if a == 0 and k < 2 else place,
+            dst_ref=place,
+            send_sem=tp_send.at[a, k],
+            recv_sem=tp_recv.at[a, k],
+            device_id={"tp": target},
+            device_id_type=MESH,
+        )
+
+    def tp_first(a):
+        tp_copy(a, 1).start()
+        tp_copy(a, 0).start()
+
+    def tp_second(a):
+        tp_copy(a, 1).wait_recv()
+        tp_copy(a, 2).start()
+
+    def tp_finish(a):
+        tp_copy(a, 0).wait_recv()
+        tp_copy(a, 2).wait_recv()
+
+    own_tokens = pltpu.make_async_copy(tokens, tp_slot(0, tp), local_sem.at[6])
+    tp_first(0)
+    own_tokens.start()
+    for w in (1, 2, 0, 3):
+        first(w)
+    second(1)
+    second(2)
+    second(0)
+    first(4)
+    third(1)
+    third(2)
+    third(0)
+    second(3)
+    first(5)
+    tp_second(0)
+    finish(2)
+    tp_first(2)
+    finish(1)
+    tp_finish(0)
+    own_tokens.wait()
+
+    count = tokens.shape[0] // ROWS
+    chan = mixed.shape[1] // TP
+
+    def tile(i):
+        return pl.ds(pl.multiple_of(i * ROWS, ROWS), ROWS)
+
+    def normalised(values, gain):
+        inverse = lax.rsqrt(jnp.mean(values * values, axis=-1, keepdims=True) + 1e-06)
+        return (values * inverse * gain[...]).astype(bf16)
+
+    @pl.loop(0, count)
+    def _(i):
+        normed = normalised(rows[tile(i), :].astype(f32), mixer_gain)
+        three = jnp.dot(normed, mixer[...], preferred_element_type=f32) * s_mixer[...]
+        product = three[:, chan : 2 * chan] * three[:, 2 * chan :]
+        place = lax.rem(lax.broadcasted_iota(jnp.int32, product.shape, 0), SEQ_LEN)
+        total = jnp.zeros_like(product)
+        last = taps.shape[0] - 1
+        for j in range(taps.shape[0]):
+            back = last - j
+            moved = product
+            if back:
+                moved = jnp.where(place >= back, pltpu.roll(product, back, 0), 0.0)
+            total = total + taps[j : j + 1, :] * moved
+        mixed[tile(i), pl.ds(pl.multiple_of(tp * chan, chan), chan)] = (
+            three[:, :chan] * total
+        ).astype(bf16)
+
+    tp_first(1)
+    third(3)
+    second(4)
+    tp_second(2)
+    tp_second(1)
+    finish(0)
+    tp_finish(2)
+    tp_finish(1)
+    for k in range(3):
+        tp_copy(0, k).wait_send()
+
+    block = scales.shape[1]
+    blocks = DEPTH * WIDTH
+
+    def scale_row(which):
+        return jnp.concatenate(
+            [scales[b * 16 + which * 8 : b * 16 + which * 8 + 1, :] for b in range(blocks)], axis=1
+        )
+
+    feat = tokens.shape[1]
+
+    @pl.loop(0, count)
+    def _(i):
+        term = jnp.dot(mixed[tile(i), :], mixout[...], preferred_element_type=f32) * scale_row(0)
+        residual = (rows[tile(i), :].astype(f32) + term).astype(bf16)
+        rows[tile(i), :] = residual
+        residual_own[tile(i), :] = rows[tile(i), pl.ds(pl.multiple_of(tp * feat, feat), feat)]
+        rows[tile(i), :] = normalised(residual.astype(f32), ffn_gain)
+
+    third(4)
+    second(5)
+    finish(3)
+    finish(4)
+
+    @pl.loop(0, count)
+    def _(i):
+        gate_part = jnp.dot(rows[tile(i), :], gate[...], preferred_element_type=f32) * s_gate[...]
+        up_part = jnp.dot(rows[tile(i), :], up[...], preferred_element_type=f32) * s_up[...]
+        hidden[tile(i), :] = (gate_part / (1.0 + jnp.exp(-gate_part)) * up_part).astype(bf16)
+
+    third(5)
+    finish(5)
+
+    @pl.loop(0, count)
+    def _(i):
+        term = jnp.dot(hidden[tile(i), :], down[...], preferred_element_type=f32) * scale_row(1)
+        out[tile(i), :] = term.astype(bf16)
+
+    for w in range(6):
+        for k in range(9):
+            copy(w, k).wait_send()
+    for a in (1, 2):
+        for k in range(3):
+            tp_copy(a, k).wait_send()
+
+
+def fused_device(
+    tokens,
+    mixer_gain,
+    ffn_gain,
+    w_outer,
+    w_inner,
+    w_value,
+    scale_outer,
+    scale_inner,
+    scale_value,
+    conv_taps,
+    w_mixout,
+    scale_mixout,
+    w_gate,
+    w_upward,
+    scale_gate,
+    scale_upward,
+    w_down,
+    scale_down,
+):
+    bf16 = jnp.bfloat16
+    count, feat = tokens.shape
+    model = mixer_gain.shape[0]
+    chan = w_outer.shape[1]
+    units = w_gate.shape[1]
+    cols = w_down.shape[1]
+    shard = jnp.concatenate([w_outer, w_inner, w_value], axis=1).astype(bf16)
+    s_mixer = jnp.concatenate([scale_outer, scale_inner, scale_value], axis=1)
+    scale_shard = jnp.concatenate(
+        [jnp.broadcast_to(scale_mixout, (8, cols)), jnp.broadcast_to(scale_down, (8, cols))], axis=0
+    )
+    vmem = pl.BlockSpec(memory_space=pltpu.VMEM)
+    dma = pltpu.SemaphoreType.DMA
+    terms, residual = pl.pallas_call(
+        block_kernel,
+        out_shape=(
+            jax.ShapeDtypeStruct((count, model), bf16),
+            jax.ShapeDtypeStruct((count, feat), bf16),
+        ),
+        in_specs=[vmem] * 13,
+        out_specs=(vmem, vmem),
+        scratch_shapes=[
+            pltpu.VMEM((count, model), bf16),
+            pltpu.VMEM((model, 3 * chan), bf16),
+            pltpu.VMEM((TP * chan, model), bf16),
+            pltpu.VMEM((model, units), bf16),
+            pltpu.VMEM((model, units), bf16),
+            pltpu.VMEM((units, model), bf16),
+            pltpu.VMEM((16 * DEPTH * WIDTH, cols), jnp.float32),
+            pltpu.VMEM((count, TP * chan), bf16),
+            pltpu.VMEM((count, units), bf16),
+            dma((6, 9)),
+            dma((6, 9)),
+            dma((3, 3)),
+            dma((3, 3)),
+            dma((7,)),
+        ],
+        compiler_params=pltpu.CompilerParams(
+            collective_id=0, has_side_effects=True, vmem_limit_bytes=62 * 1024 * 1024
+        ),
+    )(
+        tokens, mixer_gain[None], ffn_gain[None], s_mixer, conv_taps, scale_gate, scale_upward,
+        scale_shard, shard, w_mixout.astype(bf16), w_gate.astype(bf16), w_upward.astype(bf16),
+        w_down.astype(bf16),
+    )
+    share = lax.psum_scatter(terms, "tp", scatter_dimension=1, tiled=True)
+    return (residual.astype(jnp.float32) + share.astype(jnp.float32)).astype(bf16)
+
+
+def plain_device(
     tokens,
     mixer_gain,
     ffn_gain,
@@ -122,6 +428,7 @@
         P(None, "fs"),
     )
     out_specs = P("fs", "tp")
+    chosen = fused_device if (mesh.shape["fs"], mesh.shape["tp"]) == (8, 4) else plain_device
     return jax.shard_map(
-        per_device, mesh=mesh, in_specs=in_specs, out_specs=out_specs, check_vma=False
-    )
+        chosen, mesh=mesh, in_specs=in_specs, out_specs=out_specs, check_vma=False
+    )

time: 624 us -> 380 us (0.61)
  waiting for transfers between devices: 500 us -> 47 us
  Pallas kernels: 0 us -> 308 us
  matrix products: 56.6 us -> 0 us
  blocking collectives: 34.8 us -> 0 us
    all_gather x10 -> x0, waiting for transfers between devices: 456 us -> none  [the longest x1 93.2 us: per_device(): lax.all_gather(w_down.astype(jnp.bfloat16), 'fs', axis=1, tiled=True)]
    pallas_call x0 -> x1, Pallas kernels: none -> 308 us  [fused_device(): pl.pallas_call(block_kernel, out_shape=(jax.ShapeDtypeStruct((count, mode...]
    dot_general x6 -> x0, matrix products: 56.6 us -> none  [the longest x4 24.7 us: add_rows(): return jnp.dot(left, w_piece, preferred_element_type=jnp.float32)]
    all_gather x2 -> x0, blocking collectives: 34.8 us -> none  [the longest x1 18.2 us: per_device(): lax.all_gather(scale_mixout, 'fs', axis=1, tiled=True)]
    convert_element_type x8 -> x5, other arithmetic: 13.6 us -> 6.94 us  [the longest x1 2.48 us: fused_device(): (residual.astype(jnp.float32) + share.astype(jnp.float32)).astype(bf16)]
  transfers between devices with their start and end apart: 11 -> 1, of which waited for: 10 -> 1; matrix products, arithmetic and copies ran while one was open for 8% -> 0% of each run, Pallas kernels for 0% -> 0%
where the time goes in v1:
time: 380 us
  Pallas kernels  308 us (81%)
  waiting for transfers between devices  47 us (12%)
  between operations  13.4 us (4%)
  other arithmetic  12 us (3%)
    pallas_call x1, Pallas kernels, fused_device(): pl.pallas_call(block_kernel, out_shape=(jax.ShapeDtypeStruct((count, mode...  308 us
    reduce_scatter x1, waiting for transfers between devices, fused_device(): share = lax.psum_scatter(terms, 'tp', scatter_dimension=1, tiled=True)  47 us
  transfers between devices with their start and end apart: 1, of which 1 were waited for; matrix products, arithmetic and copies ran while one was open for 0% of the time, Pallas kernels for 0%

profile of v1, /device:TPU:0, one launch (start us, length us, event | category | flops | bytes accessed | tf_op | source)
XLA Modules:
  0.0 380.2 jit_solution(11508268790806069277)
XLA Ops:
  6.5 0.0 copy-start
  6.5 0.0 copy-start.1
  6.5 0.0 reduce-scatter.2.cloned.1.call-start
  6.5 1.1 convert.9
  7.7 1.0 convert.10
  8.6 1.0 convert.11
  9.6 1.6 convert_element_type.22.h_mixout
  11.2 0.0 copy-done
  11.2 0.0 copy-start.2
  11.2 0.9 convert_element_type.23.h_gate
  12.2 0.0 copy-done.1
  12.2 0.0 copy-start.4
  12.2 0.0 copy-start.5
  12.2 0.0 copy-start.7
  12.2 0.0 copy-start.8
  12.2 1.0 convert_element_type.24.h_up
  13.2 0.0 copy-done.2
  13.2 0.9 convert_element_type.25.h_down
  14.1 0.0 copy-done.4
  14.1 0.0 copy-done.5
  14.1 0.6 pad_maximum_fusion.1.h_scales
  14.7 0.0 copy-done.6
  14.7 0.0 copy-done.7
  14.7 0.0 copy-done.8
  14.7 0.6 pad_maximum_fusion.2.s_mixer
  15.3 0.8 pad_maximum_fusion.h_mixer
  16.1 307.7 %shard_map.172 = (bf16[1024,2048]{1,0:T(8,128)(2,1)}, bf16[1024,512]{1,0:T(8,128)(2,1)}) custom-call(bf16[1024,512]{1,0:T(8,128)(2,1)} %tokens.1, f32[1,2048]{1,0:T(1,128)} %bitcast.4, f32[1,2048]{1,0:T(1,128)} %bitcast.5, f32[1,768]{1,0:T(1,128)} %pad_maximum_fusion.2.s_mixer, f32[3,256]{1,0:T(4,128)} %taps.1, f32[1,1408]{1,0:T(1,128)} %s_gate.1, ...), custom_call_target="tpu_custom_call" | custom-call | tf_op jit(solution)/shard_map/pallas_call | solution.py:298
  323.9 0.0 copy-start.3
  323.9 0.0 reduce-scatter.2.cloned.1.call-update
  323.9 47.0 %reduce-scatter.2.cloned.1.call-done = bf16[1024,512]{1,0:T(8,128)(2,1)} async-done(((bf16[1024,2048]{1,0:T(8,128)(2,1)}), bf16[1024,512]{1,0:T(8,128)(2,1)}) %reduce-scatter.2.cloned.1.call-update) | async-done | bytes 1048592 | tf_op jit(solution)/shard_map/reduce_scatter | solution.py:330
  370.9 0.0 copy-done.3
  370.9 2.5 add_convert_fusion
  (3 shorter events, 0.0 us)
Async XLA Ops:
  6.5 4.7 %copy-start = (f32[256,1408]{1,0:T(8,128)S(1)}, f32[256,1408]{1,0:T(8,128)}, u32[]{:S(2)}) copy-start(f32[256,1408]{1,0:T(8,128)} %param.30) | copy-start | bytes 4325380
  6.5 5.6 %copy-start.1 = (f32[256,1408]{1,0:T(8,128)S(1)}, f32[256,1408]{1,0:T(8,128)}, u32[]{:S(2)}) copy-start(f32[256,1408]{1,0:T(8,128)} %param.31) | copy-start | bytes 4325380
  6.5 364.3 %reduce-scatter.2.cloned.1.call-start = ((), (), s32[]{:S(2)}) async-start(), calls=%async_computation.1 | async-start | bytes 5242880 | tf_op jit(solution)/shard_map/reduce_scatter | solution.py:330
  11.2 1.9 copy-start.2
  12.2 1.9 copy-start.4
  12.2 1.9 copy-start.5
  12.2 2.6 copy-start.6
  12.2 2.6 copy-start.7
  12.2 2.5 copy-start.8
  323.9 47.0 %copy-start.3 = (bf16[1024,512]{1,0:T(8,128)(2,1)S(1)}, bf16[1024,512]{1,0:T(8,128)(2,1)}, u32[]{:S(2)}) copy-start(bf16[1024,512]{1,0:T(8,128)(2,1)} %get-tuple-element.7) | copy-start | bytes 3145732
Sparse Core Ops, SparseCore 0:
  324.0 46.7 reduce-scatter.1
